TPU v7x, 32 devices: a whole 2x2x4 slice. The times are simulated.
32 devices in a mesh: sp: 8 (over z, y), tp: 4 (over x, core).
Axes of the slice: x: 2, y: 2, z: 4, core: 2. Of those that a mesh axis runs over, the one named last changes fastest.
Arguments:
- query_a: bfloat16 [1536, 2048], P('sp', 'tp'), may hold values from -7.5 to 7.5
- key_a: bfloat16 [1536, 1024], P('sp', 'tp'), may hold values from -7.5 to 7.5
- value_a: bfloat16 [1536, 1024], P('sp', 'tp'), may hold values from -6 to 6
- query_b: bfloat16 [1536, 2048], P('sp', 'tp'), may hold values from -7.5 to 7.5
- key_b: bfloat16 [1536, 512], P('sp', 'tp'), may hold values from -7.5 to 7.5
- value_b: bfloat16 [1536, 512], P('sp', 'tp'), may hold values from -6 to 6
- gain_a: float32 [2, 128], replicated, may hold values from 1 to 6.5
- gain_b: float32 [2, 64], replicated, may hold values from 1 to 8.5
- out_a: bfloat16 [2048, 4096], P('tp'), may hold values from -0.5 to 0.5
- out_b: bfloat16 [2048, 4096], P('tp'), may hold values from -0.5 to 0.5
- residual: bfloat16 [1536, 4096], P('sp'), may hold values from -6 to 6
- norm_gain: float32 [4096], replicated, may hold values from 0.1 to 1.9
- gate_weight: bfloat16 [4096, 6144], P('sp', 'tp'), may hold values from -0.09375 to 0.09375
- up_weight: bfloat16 [4096, 6144], P('sp', 'tp'), may hold values from -0.09375 to 0.09375
- down_weight: bfloat16 [6144, 4096], P('tp', 'sp'), may hold values from -0.3125 to 0.3125
Outputs:
- output: bfloat16 [1536, 4096], P(('sp', 'tp'))
All inputs are finite; a program needn't handle non-finite values.
Results may differ from a plain program's by a relative error of at most 0.017.
The roundings to bfloat16 on the way count: a program that leaves them out, or rounds other values in their place, can miss the bound.
Values may be sent and summed in bfloat16 or wider, within the bound.
A program may use at most 128 MiB of HBM per device.

v0:
```python
import jax
import jax.numpy as jnp
from jax import lax
from jax.sharding import PartitionSpec as P

HEAD_A = 128
HEAD_B = 64
GRID_W = 64
epsilon = 1e-06
theta_base = 10000.0


def rotate(inputs, num_heads, head_size, first_pos, gain):
    tok_rows = inputs.shape[0]
    vectors = inputs.astype(jnp.float32).reshape(tok_rows, num_heads, head_size)
    vectors = (
        vectors * lax.rsqrt(jnp.mean(vectors * vectors, axis=-1, keepdims=True) + epsilon) * gain
    )
    position = first_pos + jnp.arange(tok_rows, dtype=jnp.int32)
    grid_row = (position // GRID_W).astype(jnp.float32)
    grid_col = (position % GRID_W).astype(jnp.float32)
    quarter = head_size // 4
    inv_freq = theta_base ** (-4.0 * jnp.arange(quarter, dtype=jnp.float32) / head_size)
    angle_row = grid_row[:, None] * inv_freq[None, :]
    angle_col = grid_col[:, None] * inv_freq[None, :]
    angles = jnp.concatenate([angle_row, angle_row, angle_col, angle_col], axis=-1)
    quarters = vectors.reshape(tok_rows, num_heads, 4, quarter)
    rotated = jnp.stack(
        [-quarters[:, :, 1], quarters[:, :, 0], -quarters[:, :, 3], quarters[:, :, 2]], axis=2
    )
    rotated = rotated.reshape(tok_rows, num_heads, head_size)
    result = vectors * jnp.cos(angles)[:, None, :] + rotated * jnp.sin(angles)[:, None, :]
    return result.reshape(tok_rows, num_heads * head_size).astype(jnp.bfloat16)


def start_state(kv_heads, groups, tok_rows, head_size):
    return (
        jnp.full((kv_heads, groups, tok_rows), -1e30, jnp.float32),
        jnp.zeros((kv_heads, groups, tok_rows), jnp.float32),
        jnp.zeros((kv_heads, groups, tok_rows, head_size), jnp.float32),
    )


def attend(state, queries, key_rows, values, head_size):
    run_max, run_sum, run_acc = state
    kv_heads = key_rows.shape[1] // head_size
    groups = run_max.shape[1]
    q_heads = queries.reshape(queries.shape[0], kv_heads, groups, head_size)
    k_heads = key_rows.reshape(key_rows.shape[0], kv_heads, head_size)
    v_heads = values.reshape(values.shape[0], kv_heads, head_size)
    scores = jnp.einsum(
        "tkgd,pkd->kgtp", q_heads, k_heads, preferred_element_type=jnp.float32
    ) * head_size ** (-0.5)
    new_max = jnp.maximum(run_max, jnp.max(scores, axis=-1))
    exp_scores = jnp.exp(scores - new_max[..., None])
    new_sum = jnp.sum(exp_scores, axis=-1)
    new_acc = jnp.einsum(
        "kgtp,pkd->kgtd",
        exp_scores.astype(jnp.bfloat16),
        v_heads,
        preferred_element_type=jnp.float32,
    )
    return (new_max, new_sum, new_acc)


def finish(state, num_cols):
    blended = state[2] / state[1][..., None]
    return blended.transpose(2, 0, 1, 3).reshape(blended.shape[2], num_cols).astype(jnp.bfloat16)


def normalize(mixed_rows, gain):
    scale = lax.rsqrt(jnp.mean(mixed_rows * mixed_rows, axis=-1, keepdims=True) + epsilon)
    return (mixed_rows * scale * gain).astype(jnp.bfloat16)


def on_device(
    query_a,
    key_a,
    value_a,
    query_b,
    key_b,
    value_b,
    gain_a,
    gain_b,
    out_a,
    out_b,
    residual,
    norm_gain,
    gate_weight,
    up_weight,
    down_weight,
):
    tok_rows = query_a.shape[0]
    first_pos = lax.axis_index("sp") * tok_rows
    heads_a = query_a.shape[1] // HEAD_A
    heads_b = query_b.shape[1] // HEAD_B
    kv_heads_a = key_a.shape[1] // HEAD_A
    kv_heads_b = key_b.shape[1] // HEAD_B
    kv_width_b = kv_heads_b * HEAD_B
    turned_qa = rotate(query_a, heads_a, HEAD_A, first_pos, gain_a[0])
    turned_ka = rotate(key_a, kv_heads_a, HEAD_A, first_pos, gain_a[1])
    turned_qb = rotate(query_b, heads_b, HEAD_B, first_pos, gain_b[0])
    turned_kb = rotate(key_b, kv_heads_b, HEAD_B, first_pos, gain_b[1])
    pair_b = jnp.concatenate([turned_kb, value_b], axis=1)
    initial = (
        start_state(kv_heads_a, heads_a // kv_heads_a, tok_rows, HEAD_A),
        start_state(kv_heads_b, heads_b // kv_heads_b, tok_rows, HEAD_B),
    )
    pieces = (
        lax.all_gather(turned_ka, "sp", axis=0, tiled=True),
        lax.all_gather(value_a, "sp", axis=0, tiled=True),
        lax.all_gather(pair_b, "sp", axis=0, tiled=True),
    )
    state_a = attend(initial[0], turned_qa, pieces[0], pieces[1], HEAD_A)
    state_b = attend(
        initial[1], turned_qb, pieces[2][:, :kv_width_b], pieces[2][:, kv_width_b:], HEAD_B
    )
    attn_a = finish(state_a, query_a.shape[1])
    attn_b = finish(state_b, query_b.shape[1])
    own_rows = tok_rows // lax.axis_size("tp")
    own_start = lax.axis_index("tp") * own_rows
    head_sum = lax.psum(
        (
            jnp.dot(attn_a, out_a, preferred_element_type=jnp.float32)
            + jnp.dot(attn_b, out_b, preferred_element_type=jnp.float32)
        ).astype(jnp.bfloat16),
        "tp",
    ).astype(jnp.float32)
    whole_mixed = residual.astype(jnp.float32) + head_sum
    normed = normalize(whole_mixed, norm_gain)
    mixed_rows = lax.dynamic_slice_in_dim(whole_mixed, own_start, own_rows, 0)
    pieces = (
        lax.all_gather(gate_weight, "sp", axis=0, tiled=True),
        lax.all_gather(up_weight, "sp", axis=0, tiled=True),
    )
    gate_act = jnp.dot(normed, pieces[0], preferred_element_type=jnp.float32)
    up_act = jnp.dot(normed, pieces[1], preferred_element_type=jnp.float32)
    hidden = (jax.nn.silu(gate_act) * up_act).astype(jnp.bfloat16)
    down_all = jnp.dot(
        hidden,
        lax.all_gather(down_weight, "sp", axis=1, tiled=True),
        preferred_element_type=jnp.float32,
    )
    branch_sum = lax.psum_scatter(
        down_all.astype(jnp.bfloat16), "tp", scatter_dimension=0, tiled=True
    ).astype(jnp.float32)
    return (mixed_rows + 0.5 * branch_sum).astype(jnp.bfloat16)


def solution(mesh):
    return jax.shard_map(
        on_device,
        mesh=mesh,
        in_specs=(
            P("sp", "tp"),
            P("sp", "tp"),
            P("sp", "tp"),
            P("sp", "tp"),
            P("sp", "tp"),
            P("sp", "tp"),
            P(),
            P(),
            P("tp", None),
            P("tp", None),
            P("sp", None),
            P(),
            P("sp", "tp"),
            P("sp", "tp"),
            P("tp", "sp"),
        ),
        out_specs=P(("sp", "tp"), None),
        check_vma=False,
    )
```

profile of v0, /device:TPU:0, one launch (start us, length us, event | category | flops | bytes accessed | tf_op | source)
XLA Modules:
  0.0 724.6 jit_solution(1680261890716808169)
XLA Ops:
  7.4 1.0 copy.39
  8.4 0.8 slice_reduce_fusion
  9.5 0.9 copy.40
  10.9 33.9 %all_gather.20 = bf16[1536,256]{1,0:T(8,128)(2,1)S(1)} all-gather(bf16[192,256]{1,0:T(8,128)(2,1)S(1)} %copy.41), channel_id=1, replica_groups=mesh['sp'=8,'tp'=4] {'sp'}, dimensions={0}, use_global_device_ids=true | all-gather | bytes 884736 | tf_op jit(solution)/shard_map/all_gather | solution.py:112
  45.8 5.1 bitcast_reduce_fusion
  52.1 0.2 fusion.46
  52.6 32.3 %all_gather.18 = bf16[1536,256]{1,0:T(8,128)(2,1)S(1)} all-gather(bf16[192,256]{1,0:T(8,128)(2,1)S(1)} %copy.31), channel_id=1, replica_groups=mesh['sp'=8,'tp'=4] {'sp'}, dimensions={0}, use_global_device_ids=true | all-gather | bytes 884736 | tf_op jit(solution)/shard_map/all_gather | solution.py:110
  84.9 0.3 copy.32
  85.5 3.1 bitcast_reduce_fusion.1
  88.5 32.2 %all_gather.19 = bf16[1536,256]{1,0:T(8,128)(2,1)S(1)} all-gather(bf16[192,256]{1,0:T(8,128)(2,1)S(1)} %copy-done.6), channel_id=1, replica_groups=mesh['sp'=8,'tp'=4] {'sp'}, dimensions={0}, use_global_device_ids=true | all-gather | bytes 884736 | tf_op jit(solution)/shard_map/all_gather | solution.py:111
  120.7 0.3 copy.36
  121.0 3.4 fusion.7
  124.4 0.3 copy-done
  124.8 1.0 fusion.23
  126.1 5.4 fusion.1
  131.5 5.7 fusion.29
  137.2 1.0 fusion.57
  138.2 1.2 copy-done.2
  139.4 2.2 fusion.3
  141.7 0.5 all-gather.4.cloned.1.call-update
  142.2 0.5 all-gather.6.cloned.1.call-update
  142.8 0.5 all-gather.8.cloned.1.call-update
  143.4 0.3 reduce-scatter.2.cloned.1.call-start
  143.6 41.4 %all-reduce.2.cloned.1.call-done = bf16[192,4096]{1,0:T(8,128)(2,1)} async-done(((bf16[192,4096]{1,0:T(8,128)(2,1)}), bf16[192,4096]{1,0:T(8,128)(2,1)}) %all-reduce.2.cloned.1.call-update) | async-done | bytes 1572880 | tf_op jit(solution)/shard_map/psum | solution.py:122
  185.1 2.5 convert_add_fusion
  187.6 133.1 %all-gather.4.cloned.1.call-done = bf16[4096,1536]{1,0:T(8,128)(2,1)} async-done(((bf16[512,1536]{1,0:T(8,128)(2,1)}), bf16[4096,1536]{1,0:T(8,128)(2,1)}) %all-gather.4.cloned.1.call-update) | async-done | bytes 12582928 | tf_op jit(solution)/shard_map/all_gather | solution.py:133
  320.7 9.2 %fusion.55 = f32[192,1536]{1,0:T(8,128)} fusion(bf16[4096,1536]{1,0:T(8,128)(2,1)} %all-gather.4.cloned.1.call-done, f32[4096]{0:T(1024)S(1)} %copy-done.8, f32[192]{0:T(256)S(1)} %add_rsqrt_fusion.4, bf16[192,4096]{1,0:T(8,128)(2,1)} %all-reduce.2.cloned.1.call-done, bf16[192,4096]{1,0:T(8,128)(2,1)} %param.25), kind=kOutput, calls=%fused_computation.121 | convolution fusion | flops 2420637696 | bytes 16925440 | tf_op jit(solution)/shard_map/dot_general | solution.py:136
  329.9 167.0 %all-gather.6.cloned.1.call-done = bf16[4096,1536]{1,0:T(8,128)(2,1)} async-done(((bf16[512,1536]{1,0:T(8,128)(2,1)}), bf16[4096,1536]{1,0:T(8,128)(2,1)}) %all-gather.6.cloned.1.call-update) | async-done | bytes 12582928 | tf_op jit(solution)/shard_map/all_gather | solution.py:134
  496.9 176.0 %all-gather.8.cloned.1.call-done = bf16[1536,4096]{1,0:T(8,128)(2,1)} async-done(((bf16[1536,512]{1,0:T(8,128)(2,1)}), bf16[1536,4096]{1,0:T(8,128)(2,1)}) %all-gather.8.cloned.1.call-update) | async-done | bytes 12582928 | tf_op jit(solution)/shard_map/all_gather | solution.py:141
  672.9 15.9 %convolution_convert_fusion = bf16[192,4096]{1,0:T(8,128)(2,1)} fusion(bf16[1536,4096]{1,0:T(8,128)(2,1)} %all-gather.8.cloned.1.call-done, bf16[4096,1536]{1,0:T(8,128)(2,1)} %all-gather.6.cloned.1.call-done, f32[192,1536]{1,0:T(8,128)} %fusion.55, f32[4096]{0:T(1024)S(1)} %copy-done.8, f32[192]{0:T(256)S(1)} %add_rsqrt_fusion.4, ...), kind=kOutput, calls=%fused_computation.7 | convolution fusion | flops 4839112704 | bytes 31081216 | tf_op jit(solution)/shard_map/dot_general | solution.py:139
  688.8 26.4 %reduce-scatter.2.cloned.1.call-done = bf16[48,4096]{1,0:T(8,128)(2,1)} async-done(((bf16[192,4096]{1,0:T(8,128)(2,1)}), bf16[48,4096]{1,0:T(8,128)(2,1)}) %reduce-scatter.2.cloned.1.call-update) | async-done | bytes 393232 | tf_op jit(solution)/shard_map/reduce_scatter | solution.py:144
  715.2 1.8 add_convert_fusion
  (77 shorter events, 3.8 us)
Async XLA Ops:
  7.4 37.6 %copy-start.3 = (bf16[192,512]{1,0:T(8,128)(2,1)S(1)}, bf16[192,512]{1,0:T(8,128)(2,1)}, u32[]{:S(2)}) copy-start(bf16[192,512]{1,0:T(8,128)(2,1)} %param.18) | copy-start | bytes 589828
  7.4 177.7 %all-reduce.2.cloned.1.call-start = ((), (), s32[]{:S(2)}) async-start(), calls=%async_computation.1 | async-start | bytes 3145728 | tf_op jit(solution)/shard_map/psum | solution.py:122
  45.8 5.3 copy-start.4
  45.8 5.5 copy-start.7
  50.9 0.9 copy-start.5
  85.4 3.1 copy-start.6
  121.0 3.8 copy-start
  131.4 5.7 copy-start.1
  137.2 2.2 copy-start.2
  141.6 179.1 %all-gather.4.cloned.1.call-start = ((), (), s32[]{:S(2)}) async-start(), calls=%async_computation.2 | async-start | bytes 14155776 | tf_op jit(solution)/shard_map/all_gather | solution.py:133
  142.2 354.7 %all-gather.6.cloned.1.call-start = ((), (), s32[]{:S(2)}) async-start(), calls=%async_computation.3 | async-start | bytes 14155776 | tf_op jit(solution)/shard_map/all_gather | solution.py:134
  142.8 530.2 %all-gather.8.cloned.1.call-start = ((), (), s32[]{:S(2)}) async-start(), calls=%async_computation.4 | async-start | bytes 14155776 | tf_op jit(solution)/shard_map/all_gather | solution.py:141
  143.4 177.3 %copy-start.8 = (f32[4096]{0:T(1024)S(1)}, f32[4096]{0:T(1024)}, u32[]{:S(2)}) copy-start(f32[4096]{0:T(1024)} %param.26) | copy-start | bytes 49156
  143.4 571.8 %reduce-scatter.2.cloned.1.call-start = ((), (), s32[]{:S(2)}) async-start(), calls=%async_computation.5 | async-start | bytes 1966080 | tf_op jit(solution)/shard_map/reduce_scatter | solution.py:144
Sparse Core Ops, SparseCore 0:
  141.7 43.2 all-reduce.1
  688.9 26.2 reduce-scatter.1
Sparse Core Ops, SparseCore 1:
  144.3 176.3 all-gather.3
  322.8 174.1 all-gather.5
  498.8 174.1 all-gather.7
where the time goes:
time: 725 us
  waiting for transfers between devices  546 us (75%)
  blocking collectives  98.4 us (14%)
  matrix products  43.1 us (6%)
  between operations  15.4 us (2%)
  other arithmetic  15.1 us (2%)
    all_gather x1, waiting for transfers between devices, on_device(): lax.all_gather(down_weight, 'sp', axis=1, tiled=True)  176 us
    all_gather x1, waiting for transfers between devices, on_device(): lax.all_gather(up_weight, 'sp', axis=0, tiled=True)  167 us
    all_gather x1, waiting for transfers between devices, on_device(): lax.all_gather(gate_weight, 'sp', axis=0, tiled=True)  133 us
    psum x1, waiting for transfers between devices, on_device(): lax.psum((jnp.dot(attn_a, out_a, preferred_element_type=jnp.float32) + jn...  41.4 us
    all_gather x1, blocking collectives, on_device(): lax.all_gather(pair_b, 'sp', axis=0, tiled=True)  33.9 us
    all_gather x1, blocking collectives, on_device(): lax.all_gather(turned_ka, 'sp', axis=0, tiled=True)  32.3 us
    all_gather x1, blocking collectives, on_device(): lax.all_gather(value_a, 'sp', axis=0, tiled=True)  32.2 us
    reduce_scatter x1, waiting for transfers between devices, on_device(): lax.psum_scatter(down_all.astype(jnp.bfloat16), 'tp', scatter_dimension=0...  26.4 us
  transfers between devices with their start and end apart: 5, of which 5 were waited for; matrix products, arithmetic and copies ran while one was open for 2% of the time, Pallas kernels for 0%

commit v1 on v0

--- a/solution.py
+++ b/solution.py
@@ -119,12 +119,15 @@
     attn_b = finish(state_b, query_b.shape[1])
     own_rows = tok_rows // lax.axis_size("tp")
     own_start = lax.axis_index("tp") * own_rows
-    head_sum = lax.psum(
-        (
-            jnp.dot(attn_a, out_a, preferred_element_type=jnp.float32)
-            + jnp.dot(attn_b, out_b, preferred_element_type=jnp.float32)
-        ).astype(jnp.bfloat16),
-        "tp",
+    head_sum = jnp.sum(
+        lax.all_gather(
+            (
+                jnp.dot(attn_a, out_a, preferred_element_type=jnp.float32)
+                + jnp.dot(attn_b, out_b, preferred_element_type=jnp.float32)
+            ).astype(jnp.bfloat16),
+            "tp",
+        ),
+        axis=0,
     ).astype(jnp.float32)
     whole_mixed = residual.astype(jnp.float32) + head_sum
     normed = normalize(whole_mixed, norm_gain)

time: 725 us -> 769 us (1.061)
  waiting for transfers between devices: 546 us -> 589 us
    all_gather x0 -> x1, waiting for transfers between devices: none -> 44.5 us  [on_device(): lax.all_gather((jnp.dot(attn_a, out_a, preferred_element_type=jnp.float32...]
    psum x1 -> x0, waiting for transfers between devices: 41.4 us -> none  [on_device(): lax.psum((jnp.dot(attn_a, out_a, preferred_element_type=jnp.float32) + jn...]
    all_gather x1, waiting for transfers between devices: 133 us -> 172 us  [on_device(): lax.all_gather(gate_weight, 'sp', axis=0, tiled=True)]
    all_gather x1, waiting for transfers between devices: 167 us -> 176 us  [on_device(): lax.all_gather(up_weight, 'sp', axis=0, tiled=True)]
    all_gather x1, waiting for transfers between devices: 176 us -> 168 us  [on_device(): lax.all_gather(down_weight, 'sp', axis=1, tiled=True)]
where the time goes in v1:
time: 769 us
  waiting for transfers between devices  589 us (77%)
  blocking collectives  98.5 us (13%)
  matrix products  41.2 us (5%)
  other arithmetic  19.3 us (3%)
  between operations  13.6 us (2%)
    all_gather x1, waiting for transfers between devices, on_device(): lax.all_gather(up_weight, 'sp', axis=0, tiled=True)  176 us
    all_gather x1, waiting for transfers between devices, on_device(): lax.all_gather(gate_weight, 'sp', axis=0, tiled=True)  172 us
    all_gather x1, waiting for transfers between devices, on_device(): lax.all_gather(down_weight, 'sp', axis=1, tiled=True)  168 us
    all_gather x1, waiting for transfers between devices, on_device(): lax.all_gather((jnp.dot(attn_a, out_a, preferred_element_type=jnp.float32...  44.5 us
    all_gather x1, blocking collectives, on_device(): lax.all_gather(pair_b, 'sp', axis=0, tiled=True)  33.9 us
    all_gather x1, blocking collectives, on_device(): lax.all_gather(turned_ka, 'sp', axis=0, tiled=True)  32.3 us
    all_gather x1, blocking collectives, on_device(): lax.all_gather(value_a, 'sp', axis=0, tiled=True)  32.3 us
    reduce_scatter x1, waiting for transfers between devices, on_device(): lax.psum_scatter(down_all.astype(jnp.bfloat16), 'tp', scatter_dimension=0...  26.4 us
  transfers between devices with their start and end apart: 5, of which 5 were waited for; matrix products, arithmetic and copies ran while one was open for 2% of the time, Pallas kernels for 0%

profile of v1, /device:TPU:0, one launch (start us, length us, event | category | flops | bytes accessed | tf_op | source)
XLA Modules:
  0.0 768.7 jit_solution(569485754671065084)
XLA Ops:
  6.6 1.0 copy.39
  7.6 0.8 slice_reduce_fusion
  8.7 0.9 copy.40
  10.0 33.9 %all_gather.26 = bf16[1536,256]{1,0:T(8,128)(2,1)S(1)} all-gather(bf16[192,256]{1,0:T(8,128)(2,1)S(1)} %copy.41), channel_id=1, replica_groups=mesh['sp'=8,'tp'=4] {'sp'}, dimensions={0}, use_global_device_ids=true | all-gather | bytes 884736 | tf_op jit(solution)/shard_map/all_gather | solution.py:112
  45.0 5.1 bitcast_reduce_fusion
  51.8 32.3 %all_gather.24 = bf16[1536,256]{1,0:T(8,128)(2,1)S(1)} all-gather(bf16[192,256]{1,0:T(8,128)(2,1)S(1)} %copy.31), channel_id=1, replica_groups=mesh['sp'=8,'tp'=4] {'sp'}, dimensions={0}, use_global_device_ids=true | all-gather | bytes 884736 | tf_op jit(solution)/shard_map/all_gather | solution.py:110
  84.2 0.3 copy.32
  84.7 3.1 bitcast_reduce_fusion.1
  87.7 32.3 %all_gather.25 = bf16[1536,256]{1,0:T(8,128)(2,1)S(1)} all-gather(bf16[192,256]{1,0:T(8,128)(2,1)S(1)} %copy-done.7), channel_id=1, replica_groups=mesh['sp'=8,'tp'=4] {'sp'}, dimensions={0}, use_global_device_ids=true | all-gather | bytes 884736 | tf_op jit(solution)/shard_map/all_gather | solution.py:111
  120.0 0.3 copy.36
  120.3 3.4 fusion.7
  123.7 0.3 copy-done
  124.1 1.0 fusion.23
  125.3 5.4 fusion.1
  130.7 5.7 fusion.29
  136.5 1.0 fusion.57
  137.5 1.2 copy-done.2
  138.7 2.2 fusion.3
  140.9 0.7 all-gather.6.cloned.1.call-update
  141.7 0.7 all-gather.10.cloned.1.call-update
  142.4 0.5 all-gather.8.cloned.1.call-update
  142.9 0.3 reduce-scatter.2.cloned.1.call-start
  143.2 44.5 %all-gather.12.cloned.1.call-done = bf16[768,4096]{1,0:T(8,128)(2,1)} async-done(((bf16[192,4096]{1,0:T(8,128)(2,1)}), bf16[768,4096]{1,0:T(8,128)(2,1)}) %all-gather.12.cloned.1.call-update) | async-done | bytes 6291472 | tf_op jit(solution)/shard_map/all_gather | solution.py:123
  187.7 4.2 reduce_sum.81
  192.0 2.1 convert_add_fusion
  194.1 171.9 %all-gather.6.cloned.1.call-done = bf16[4096,1536]{1,0:T(8,128)(2,1)} async-done(((bf16[512,1536]{1,0:T(8,128)(2,1)}), bf16[4096,1536]{1,0:T(8,128)(2,1)}) %all-gather.6.cloned.1.call-update) | async-done | bytes 12582928 | tf_op jit(solution)/shard_map/all_gather | solution.py:136
  366.0 8.3 %fusion.55 = f32[192,1536]{1,0:T(8,128)} fusion(bf16[4096,1536]{1,0:T(8,128)(2,1)} %all-gather.6.cloned.1.call-done, f32[4096]{0:T(1024)S(1)} %copy-done.9, f32[192]{0:T(256)S(1)} %add_rsqrt_fusion.4, bf16[192,4096]{1,0:T(8,128)(2,1)S(1)} %reduce_sum.81, bf16[192,4096]{1,0:T(8,128)(2,1)S(1)} %copy-done.3), kind=kOutput, calls=%fused_computation.121 | convolution fusion | flops 2420637696 | bytes 16925440 | tf_op jit(solution)/shard_map/dot_general | solution.py:139
  374.3 168.1 %all-gather.10.cloned.1.call-done = bf16[1536,4096]{1,0:T(8,128)(2,1)} async-done(((bf16[1536,512]{1,0:T(8,128)(2,1)}), bf16[1536,4096]{1,0:T(8,128)(2,1)}) %all-gather.10.cloned.1.call-update) | async-done | bytes 12582928 | tf_op jit(solution)/shard_map/all_gather | solution.py:144
  542.4 176.4 %all-gather.8.cloned.1.call-done = bf16[4096,1536]{1,0:T(8,128)(2,1)} async-done(((bf16[512,1536]{1,0:T(8,128)(2,1)}), bf16[4096,1536]{1,0:T(8,128)(2,1)}) %all-gather.8.cloned.1.call-update) | async-done | bytes 12582928 | tf_op jit(solution)/shard_map/all_gather | solution.py:137
  718.8 14.9 %convolution_convert_fusion = bf16[192,4096]{1,0:T(8,128)(2,1)} fusion(bf16[1536,4096]{1,0:T(8,128)(2,1)} %all-gather.10.cloned.1.call-done, bf16[4096,1536]{1,0:T(8,128)(2,1)} %all-gather.8.cloned.1.call-done, f32[192,1536]{1,0:T(8,128)} %fusion.55, f32[4096]{0:T(1024)S(1)} %copy-done.9, f32[192]{0:T(256)S(1)} %add_rsqrt_fusion.4, ...), kind=kOutput, calls=%fused_computation.7 | convolution fusion | flops 4839112704 | bytes 31081216 | tf_op jit(solution)/shard_map/dot_general | solution.py:142
  733.7 26.4 %reduce-scatter.2.cloned.1.call-done = bf16[48,4096]{1,0:T(8,128)(2,1)} async-done(((bf16[192,4096]{1,0:T(8,128)(2,1)}), bf16[48,4096]{1,0:T(8,128)(2,1)}) %reduce-scatter.2.cloned.1.call-update) | async-done | bytes 393232 | tf_op jit(solution)/shard_map/reduce_scatter | solution.py:147
  760.1 2.1 add_convert_fusion
  (80 shorter events, 4.1 us)
Async XLA Ops:
  6.5 37.6 %copy-start.4 = (bf16[192,512]{1,0:T(8,128)(2,1)S(1)}, bf16[192,512]{1,0:T(8,128)(2,1)}, u32[]{:S(2)}) copy-start(bf16[192,512]{1,0:T(8,128)(2,1)} %param.18) | copy-start | bytes 589828
  6.5 181.2 %all-gather.12.cloned.1.call-start = ((), (), s32[]{:S(2)}) async-start(), calls=%async_computation.5 | async-start | bytes 7864320 | tf_op jit(solution)/shard_map/all_gather | solution.py:123
  44.9 5.3 copy-start.5
  45.0 5.5 copy-start.8
  50.0 0.9 copy-start.6
  84.7 3.1 copy-start.7
  120.3 3.8 copy-start
  130.7 5.7 copy-start.1
  136.5 2.2 copy-start.2
  140.9 225.2 %all-gather.6.cloned.1.call-start = ((), (), s32[]{:S(2)}) async-start(), calls=%async_computation.1 | async-start | bytes 14155776 | tf_op jit(solution)/shard_map/all_gather | solution.py:136
  141.6 400.8 %all-gather.10.cloned.1.call-start = ((), (), s32[]{:S(2)}) async-start(), calls=%async_computation.3 | async-start | bytes 14155776 | tf_op jit(solution)/shard_map/all_gather | solution.py:144
  142.4 576.4 %all-gather.8.cloned.1.call-start = ((), (), s32[]{:S(2)}) async-start(), calls=%async_computation.2 | async-start | bytes 14155776 | tf_op jit(solution)/shard_map/all_gather | solution.py:137
  142.9 617.2 %reduce-scatter.2.cloned.1.call-start = ((), (), s32[]{:S(2)}) async-start(), calls=%async_computation.4 | async-start | bytes 1966080 | tf_op jit(solution)/shard_map/reduce_scatter | solution.py:147
  187.7 4.2 copy-start.3
  192.0 174.1 %copy-start.9 = (f32[4096]{0:T(1024)S(1)}, f32[4096]{0:T(1024)}, u32[]{:S(2)}) copy-start(f32[4096]{0:T(1024)} %param.26) | copy-start | bytes 49156
Sparse Core Ops, SparseCore 0:
  141.0 46.6 all-gather.11
  189.9 176.0 all-gather.5
  368.1 174.2 all-gather.9
  544.5 174.2 all-gather.7
  733.8 26.2 reduce-scatter.1
